TPU v7x, 32 devices: a whole 2x2x4 slice. The times are simulated.
32 devices in a mesh: ep: 8 (over z, y), tp: 4 (over x, core).
Axes of the slice: x: 2, y: 2, z: 4, core: 2. Of those that a mesh axis runs over, the one named last changes fastest.
Arguments:
- query_rows: bfloat16 [3072, 1024], P('ep', 'tp'), may hold values from -6 to 6
- key_rows: bfloat16 [3072, 512], P('ep', 'tp'), may hold values from -6 to 6
- value_rows: bfloat16 [3072, 512], P('ep', 'tp'), may hold values from -6 to 6
- break_bias: bfloat16 [3072, 16], P('ep', 'tp'), may hold values from -14 to 0
- mixer_weight: bfloat16 [1024, 2048], P('tp'), may hold values from -0.1875 to 0.1875
- mixer_gain: bfloat16 [2048], replicated, may hold values from 0.099609375 to 1.8984375
- expert_input: bfloat16 [4096, 2048], P(('ep', 'tp')), may hold values from -6 to 6
- expert_gain: bfloat16 [2048], replicated, may hold values from 0.099609375 to 1.8984375
- route_ids: int32 [4096, 2], P('ep'), may hold values from 0 to 15, all different within a row; in each aligned block of 128 rows (0 to 127, 128 to 255, ...) at most 32 rows name the same one
- route_weights: float32 [4096, 2], P(('ep', 'tp')), may hold values from 0.2 to 2
- expert_gate: bfloat16 [16, 2048, 2048], P('ep', None, 'tp'), may hold values from -0.125 to 0.125
- expert_up: bfloat16 [16, 2048, 2048], P('ep', None, 'tp'), may hold values from -0.125 to 0.125
- expert_down: bfloat16 [16, 2048, 2048], P('ep', 'tp'), may hold values from -0.125 to 0.125
- shared_gate: bfloat16 [2048, 512], replicated, may hold values from -0.125 to 0.125
- shared_up: bfloat16 [2048, 512], replicated, may hold values from -0.125 to 0.125
- shared_down: bfloat16 [512, 2048], replicated, may hold values from -0.25 to 0.25
Outputs:
- mixer_out: bfloat16 [3072, 2048], P(('ep', 'tp'))
- expert_out: bfloat16 [4096, 2048], P(('ep', 'tp'))
Inputs may be any that keep to these rules, and one draw needn't show every extreme that they name: `route_ids`: each row names 2 different experts. Within the rows of one device no expert is named more than 32 times, and in every draw some expert is named exactly 32 times within the rows of some device.
All inputs are finite; a program needn't handle non-finite values.
Results may differ from a plain program's by a relative error of at most 0.012.
Values may be sent and summed in bfloat16 or wider, within the bound.
A program may use at most 192 MiB of HBM per device.

v0:
```python
import jax
import jax.numpy as jnp
from jax import lax
from jax.sharding import PartitionSpec as P

DH = 64
TOPK = 2
SEQS = 1
norm_eps = 1e-06


def rms_scale(values, gain):
    values = values.astype(jnp.float32)
    scale = lax.rsqrt(jnp.mean(values * values, axis=-1, keepdims=True) + norm_eps)
    return (values * scale * gain.astype(jnp.float32)).astype(jnp.bfloat16)


def break_terms(queries, key_block, bias_block, query_start, key_start):
    row_count = queries.shape[0]
    heads_local = queries.shape[1] * queries.shape[2]
    key_count = key_block.shape[0]
    scores = jnp.einsum("rkgd,skd->kgrs", queries, key_block, preferred_element_type=jnp.float32)
    scores = scores.reshape(heads_local, row_count, key_count) * DH ** (-0.5)
    scores = scores + bias_block.astype(jnp.float32).T[:, None, :]
    query_pos = query_start + jnp.arange(row_count, dtype=jnp.int32)
    key_pos = key_start + jnp.arange(key_count, dtype=jnp.int32)
    visible = key_pos[None, :] < query_pos[:, None]
    keep = jnp.where(visible, -jax.nn.softplus(scores), 0.0)
    beyond = lax.cumsum(keep, axis=2, reverse=True) - keep
    return (scores, visible, keep, beyond)


def block_values(scores, visible, beyond, value_block, groups):
    heads_local, row_count, key_count = scores.shape
    kv_local = value_block.shape[1]
    weights = jnp.where(visible, jnp.exp(jax.nn.log_sigmoid(scores) + beyond), 0.0).astype(
        jnp.bfloat16
    )
    weights = weights.reshape(kv_local, groups, row_count, key_count)
    summed = jnp.einsum("kgrs,skd->kgrd", weights, value_block, preferred_element_type=jnp.float32)
    return summed.reshape(heads_local, row_count, DH)


def on_device(
    query_rows,
    key_rows,
    value_rows,
    break_bias,
    mixer_weight,
    mixer_gain,
    expert_input,
    expert_gain,
    route_ids,
    route_weights,
    expert_gate,
    expert_up,
    expert_down,
    shared_gate,
    shared_up,
    shared_down,
):
    row_count = query_rows.shape[0]
    heads_local = query_rows.shape[1] // DH
    kv_local = key_rows.shape[1] // DH
    groups = heads_local // kv_local
    queries = query_rows.reshape(row_count, kv_local, groups, DH)
    ep_size = lax.axis_size("ep")
    device = lax.axis_index("ep")
    query_start = device * row_count
    span_shards = ep_size // SEQS

    def wanted(shard):
        return (shard <= device) & (shard // span_shards == device // span_shards)

    def shard_slice(piece, index):
        return lax.dynamic_slice_in_dim(piece, index * row_count, row_count, 0)

    empty_totals = jnp.zeros((ep_size, heads_local, row_count), jnp.float32)
    empty_output = jnp.zeros((heads_local, row_count, DH), jnp.float32)
    empty_parts = jnp.zeros((ep_size, heads_local, row_count, DH), jnp.float32)
    key_piece = lax.all_gather(key_rows, "ep", axis=0, tiled=True)
    value_piece = lax.all_gather(value_rows, "ep", axis=0, tiled=True)
    bias_piece = lax.all_gather(break_bias, "ep", axis=0, tiled=True)

    def one_shard(index, current):
        parts, totals = current
        shard = index
        key_block = shard_slice(key_piece, index).reshape(row_count, kv_local, DH)
        value_block = shard_slice(value_piece, index).reshape(row_count, kv_local, DH)
        bias_block = shard_slice(bias_piece, index)

        def compute(unused):
            scores, visible, keep, beyond = break_terms(
                queries, key_block, bias_block, query_start, shard * row_count
            )
            return (
                block_values(scores, visible, beyond, value_block, groups),
                jnp.sum(keep, axis=2),
            )

        def skipped(unused):
            return (empty_output, jnp.zeros((heads_local, row_count), jnp.float32))

        block_part, total = lax.cond(wanted(shard), compute, skipped, None)
        parts = lax.dynamic_update_index_in_dim(parts, block_part, shard, 0)
        totals = lax.dynamic_update_index_in_dim(totals, total, shard, 0)
        return (parts, totals)

    parts, totals = lax.fori_loop(
        0, key_piece.shape[0] // row_count, one_shard, (empty_parts, empty_totals)
    )
    later = jnp.sum(totals, axis=0) - jnp.cumsum(totals, axis=0)
    output = jnp.sum(jnp.exp(later)[..., None] * parts, axis=0)
    attended = output.transpose(1, 0, 2).reshape(row_count, heads_local * DH).astype(jnp.bfloat16)
    block = attended
    projected = lax.psum_scatter(
        jnp.dot(block, mixer_weight, preferred_element_type=jnp.float32).astype(jnp.bfloat16),
        "tp",
        scatter_dimension=0,
        tiled=True,
    ).astype(jnp.float32)
    mixer_out = rms_scale(projected, mixer_gain)
    token_count = expert_input.shape[0]
    width = expert_input.shape[1]
    local_experts = expert_gate.shape[0]
    experts_all = local_experts * ep_size
    capacity = 2 * token_count * TOPK // experts_all
    tp_index = lax.axis_index("tp")
    normed = rms_scale(expert_input, expert_gain)
    flat = lax.dynamic_slice_in_dim(route_ids, tp_index * token_count, token_count, 0).reshape(-1)
    onehot = (flat[:, None] == jnp.arange(experts_all, dtype=jnp.int32)[None, :]).astype(jnp.int32)
    before = jnp.cumsum(onehot, axis=0) - onehot
    own_slots = flat * capacity + jnp.sum(before * onehot, axis=1)
    owners = jnp.full((experts_all * capacity,), token_count, jnp.int32)
    owners = owners.at[own_slots].set(jnp.arange(own_slots.shape[0], dtype=jnp.int32) // TOPK)
    padded = jnp.concatenate([normed, jnp.zeros((1, width), normed.dtype)], axis=0)
    outgoing = padded[owners].reshape(ep_size, local_experts, capacity, width)[None]
    arrived = lax.all_to_all(outgoing, "ep", split_axis=1, concat_axis=1, tiled=True)
    piece = lax.all_gather(arrived, "tp", axis=0, tiled=True)
    gate_proj = jnp.einsum(
        "pnecd,edf->pnecf", piece, expert_gate, preferred_element_type=jnp.float32
    )
    up_proj = jnp.einsum("pnecd,edf->pnecf", piece, expert_up, preferred_element_type=jnp.float32)
    hidden = (jax.nn.silu(gate_proj) * up_proj).astype(jnp.bfloat16)
    block = hidden
    summed = lax.psum_scatter(
        jnp.einsum(
            "pnecf,efd->pnecd", block, expert_down, preferred_element_type=jnp.float32
        ).astype(jnp.bfloat16),
        "tp",
        scatter_dimension=0,
        tiled=True,
    )
    returned = lax.all_to_all(
        summed.reshape(ep_size, local_experts * capacity, width),
        "ep",
        split_axis=0,
        concat_axis=0,
        tiled=True,
    )
    results = returned.reshape(experts_all * capacity, width)
    picked = results[own_slots].reshape(token_count, TOPK, width).astype(jnp.float32)
    routed = jnp.einsum("tk,tkd->td", route_weights, picked)
    shared_hidden = (
        jax.nn.silu(jnp.dot(normed, shared_gate, preferred_element_type=jnp.float32))
        * jnp.dot(normed, shared_up, preferred_element_type=jnp.float32)
    ).astype(jnp.bfloat16)
    expert_out = (
        routed + jnp.dot(shared_hidden, shared_down, preferred_element_type=jnp.float32)
    ).astype(jnp.bfloat16)
    return (mixer_out, expert_out)


def solution(mesh):
    return jax.shard_map(
        on_device,
        mesh=mesh,
        in_specs=(
            P("ep", "tp"),
            P("ep", "tp"),
            P("ep", "tp"),
            P("ep", "tp"),
            P("tp", None),
            P(),
            P(("ep", "tp"), None),
            P(),
            P("ep", None),
            P(("ep", "tp"), None),
            P("ep", None, "tp"),
            P("ep", None, "tp"),
            P("ep", "tp", None),
            P(),
            P(),
            P(),
        ),
        out_specs=(P(("ep", "tp"), None), P(("ep", "tp"), None)),
        check_vma=False,
    )
```

profile of v0, /device:TPU:0, one launch (start us, length us, event | category | flops | bytes accessed | tf_op | source)
XLA Modules:
  0.0 609.5 jit_solution(3167960819655452069)
XLA Ops:
  7.2 0.8 broadcast_multiply_fusion
  8.1 0.1 copy.46
  8.2 0.1 eq.40
  8.3 0.1 eq.36
  8.5 0.6 reduce-window.28
  9.1 0.2 slice_reduce_fusion
  9.3 0.1 copy.45
  9.4 0.1 mul.145
  9.7 1.4 scatter_custom_fusion
  11.1 0.7 convert_element_type.85
  11.8 1.2 fusion.41
  13.0 1.2 fusion.43
  14.3 3.3 gather_fusion
  17.7 55.5 %all_to_all.10 = bf16[1,8,2,32,2048]{4,3,0,2,1:T(8,128)(2,1)S(1)} all-to-all(bf16[1,8,2,32,2048]{4,3,0,2,1:T(8,128)(2,1)} %bitcast.134), channel_id=1, replica_groups=mesh['ep'=8,'tp'=4] {'ep'}, dimensions={1} | all-to-all | bytes 4194304 | tf_op jit(solution)/shard_map/all_to_all | solution.py:138
  73.2 1.5 copy.50
  74.8 57.4 %all-gather.2.cloned.1.call-done = bf16[4,8,2,32,2048]{4,3,1,0,2:T(8,128)(2,1)} async-done(((bf16[1,8,2,32,2048]{4,3,1,0,2:T(8,128)(2,1)}), bf16[4,8,2,32,2048]{4,3,1,0,2:T(8,128)(2,1)}) %all-gather.2.cloned.1.call-update) | async-done | bytes 8388624 | tf_op jit(solution)/shard_map/all_gather | solution.py:139
  132.1 11.0 %fusion.26 = f32[2,4,8,32,512]{4,3,2,1,0:T(8,128)} fusion(bf16[4,8,2,32,2048]{4,3,1,0,2:T(8,128)(2,1)} %all-gather.2.cloned.1.call-done, bf16[2,2048,512]{2,1,0:T(8,128)(2,1)} %param.31), kind=kOutput, calls=%fused_computation.47 | convolution fusion | flops 4294967296 | bytes 16777216 | tf_op jit(solution)/shard_map/pnecd,edf->pnecf/dot_general | solution.py:143
  143.1 15.4 %convert_bitcast_fusion.2 = bf16[4,8,2,32,2048]{4,3,1,0,2:T(8,128)(2,1)} fusion(bf16[2,512,2048]{2,1,0:T(8,128)(2,1)} %param.32, f32[2,4,8,32,512]{4,3,2,1,0:T(8,128)} %fusion.26, bf16[4,8,2,32,2048]{4,3,1,0,2:T(8,128)(2,1)} %all-gather.2.cloned.1.call-done, bf16[2,2048,512]{2,1,0:T(8,128)(2,1)} %param.30), kind=kOutput, calls=%fused_computation.45 | convolution fusion | flops 8600420352 | bytes 29360128 | tf_op jit(solution)/shard_map/pnecf,efd->pnecd/dot_general | solution.py:147
  158.6 0.8 copy-done.5
  159.4 0.1 copy.42
  159.5 0.1 copy.44
  159.7 0.2 copy.43
  159.9 32.1 %all_gather.13 = bf16[3072,4]{0,1:T(4,128)(2,1)} all-gather(bf16[384,4]{0,1:T(4,128)(2,1)S(1)} %copy-done.8), channel_id=1, replica_groups=mesh['ep'=8,'tp'=4] {'ep'}, dimensions={0}, use_global_device_ids=true | all-gather | bytes 27648 | tf_op jit(solution)/shard_map/all_gather | solution.py:83
  192.0 34.8 %all_gather.12 = bf16[3072,128]{0,1:T(8,128)(2,1)} all-gather(bf16[384,128]{0,1:T(8,128)(2,1)S(1)} %copy.42), channel_id=1, replica_groups=mesh['ep'=8,'tp'=4] {'ep'}, dimensions={0}, use_global_device_ids=true | all-gather | bytes 884736 | tf_op jit(solution)/shard_map/all_gather | solution.py:81
  226.8 34.0 %all_gather.14 = bf16[3072,128]{0,1:T(8,128)(2,1)} all-gather(bf16[384,128]{0,1:T(8,128)(2,1)S(1)} %copy.44), channel_id=1, replica_groups=mesh['ep'=8,'tp'=4] {'ep'}, dimensions={0}, use_global_device_ids=true | all-gather | bytes 884736 | tf_op jit(solution)/shard_map/all_gather | solution.py:82
  260.9 41.2 %while.18 = (s32[]{:T(128)}, f32[8,4,384,64]{2,3,1,0:T(8,128)}, f32[8,4,384]{2,1,0:T(4,128)S(1)}, s32[]{:T(128)}, s32[]{:T(128)}, /*index=5*/s32[]{:T(128)}, bf1...) while((s32[]{:T(128)}, f32[8,4,384,64]{2,3,1,0:T(8,128)}, ...), condition=%wide.region_6.7_spmd, body=%wide.region_0.6_spmd.sunk | while | flops 250984336 | bytes 43047352 | solution.py:109
  260.9 34.5 %conditional.2 = (f32[1,4,384,64]{2,3,1,0:T(8,128)S(1)}, f32[1,4,384]{2,1,0:T(4,128)S(1)}) conditional(s32[]{:T(128)} %convert_element_type.126, () %tuple.76, (s32[]{:T(128)}, s32[]{:T(128)}, bf16[3072,128]{0,1:T(8,128)(2,1)}, bf16[384,2,2,64]{0,3,2,1:T(8,128)(2,1)S(1)}, bf16[3072,4]{0,1:T(4,128)(2,1)}, /*index=5*/bf16[3072,128]{0,1:T(8,128)(2,1)}) %tuple.77), branch_computations={%region_1.1_spmd, %region_2.5_spmd} | conditional | flops 250984320 | bytes 42247824 | solution.py:104
  260.9 0.7 convert_bitcast_fusion.1
  261.6 1.0 constant_dynamic-slice_fusion
  262.6 0.1 broadcast_compare_fusion.1
  262.7 3.4 fusion.17
  266.1 0.1 copy.38
  266.3 0.3 broadcast_compare_fusion
  266.5 19.3 %fusion.2 = f32[4,384,3,128]{1,2,3,0:T(4,128)S(1)} fusion(f32[4,384,3,128]{1,3,2,0:T(8,128)} %bitcast.131, f32[4,3,128]{1,2,0:T(8,128)S(1)} %copy.38, pred[384,3,128]{0,1,2:T(4,128)(4,1)S(1)} %broadcast_compare_fusion), kind=kOutput, calls=%fused_computation.8 | output fusion | flops 80216064 | bytes 4872192 | tf_op jit(solution)/shard_map/reduce-window.10
  285.8 1.7 copy-done.1
  287.6 2.5 broadcast_add_fusion
  290.1 0.2 copy.40
  290.3 1.4 copy-done.2
  291.8 3.6 fusion.21
  295.4 0.8 constant_dynamic-update-slice_fusion.4
  296.2 0.8 constant_dynamic-update-slice_fusion.4
  297.0 0.8 constant_dynamic-update-slice_fusion.4
  297.9 0.8 constant_dynamic-update-slice_fusion.4
  298.7 0.8 constant_dynamic-update-slice_fusion.4
  299.6 0.8 constant_dynamic-update-slice_fusion.4
  300.4 0.8 constant_dynamic-update-slice_fusion.4
  301.3 0.8 constant_dynamic-update-slice_fusion.4
  302.1 2.3 multiply_reduce_fusion
  304.4 1.8 convolution_convert_fusion
  306.2 0.6 dynamic-slice
  306.8 4.8 all-reduce.4.cloned.1.call-done
  311.6 2.4 constant_dynamic-slice_fusion.2
  313.9 1.4 copy.51
  315.4 241.3 %all-to-all-start.1 = ((bf16[8,64,2048]{2,1,0:T(8,128)(2,1)}), bf16[8,64,2048]{2,1,0:T(8,128)(2,1)}, u32[]{:S(2)}, u32[]{:S(2)}) async-start(bf16[8,64,2048]{2,1,0:T(8,128)(2,1)} %bitcast.135), calls=%async_computation.2 | async-start | bytes 4194304 | tf_op jit(solution)/shard_map/all_to_all | solution.py:154
  556.6 0.2 copy.58
  556.8 2.0 fusion.62
  558.9 15.9 %reduce-scatter.5.cloned.1.call-done = bf16[96,2048]{1,0:T(8,128)(2,1)} async-done(((bf16[384,2048]{1,0:T(8,128)(2,1)}), bf16[96,2048]{1,0:T(8,128)(2,1)}) %reduce-scatter.5.cloned.1.call-update) | async-done | bytes 393232 | tf_op jit(solution)/shard_map/reduce_scatter | solution.py:116
  574.8 1.2 fusion.44
  576.0 1.9 fusion.46
  577.9 10.2 %all-to-all-done.1 = bf16[8,64,2048]{2,1,0:T(8,128)(2,1)} async-done(((bf16[8,64,2048]{2,1,0:T(8,128)(2,1)}), bf16[8,64,2048]{2,1,0:T(8,128)(2,1)}, u32[]{:S(2)}, u32[]{:S(2)}) %all-to-all-start.1) | async-done | bytes 2097184 | tf_op jit(solution)/shard_map/all_to_all | solution.py:154
  588.0 5.2 gather_fusion.1
  593.2 2.5 reshape.199
  595.8 3.5 fusion.61
  599.3 3.7 fusion.36
  (78 shorter events, 1.2 us)
Async XLA Ops:
  7.2 592.1 %copy-start = (bf16[512,2048]{1,0:T(8,128)(2,1)S(1)}, bf16[512,2048]{1,0:T(8,128)(2,1)}, u32[]{:S(2)}) copy-start(bf16[512,2048]{1,0:T(8,128)(2,1)} %param.35) | copy-start | bytes 6291460
  7.2 124.9 %all-gather.2.cloned.1.call-start = ((), (), s32[]{:S(2)}) async-start(), calls=%async_computation.4 | async-start | bytes 10485760 | tf_op jit(solution)/shard_map/all_gather | solution.py:139
  74.7 236.9 %all-reduce.4.cloned.1.call-start = ((), (), s32[]{:S(2)}) async-start(), calls=%async_computation.5 | async-start | bytes 16777216
  158.5 0.9 copy-start.5
  158.5 1.0 copy-start.6
  158.5 1.2 copy-start.4
  158.5 1.3 copy-start.8
  158.6 416.2 %reduce-scatter.5.cloned.1.call-start = ((), (), s32[]{:S(2)}) async-start(), calls=%async_computation.3 | async-start | bytes 1966080 | tf_op jit(solution)/shard_map/reduce_scatter | solution.py:116
  285.8 1.7 copy-start.1
  290.1 1.7 copy-start.2
  302.1 2.3 copy-start.3
  304.4 1.8 copy-start.10
  315.4 241.3 %copy-start.9 = (f32[128,2]{0,1:T(2,128)S(1)}, f32[128,2]{0,1:T(2,128)}, u32[]{:S(2)}) copy-start(f32[128,2]{0,1:T(2,128)} %param.29) | copy-start | bytes 3076
  315.4 241.4 %copy-start.7 = (bf16[2048]{0:T(1024)(128)(2,1)S(1)}, bf16[2048]{0:T(1024)(128)(2,1)}, u32[]{:S(2)}) copy-start(bf16[2048]{0:T(1024)(128)(2,1)} %param.25) | copy-start | bytes 12292
  315.4 272.7 %all-to-all-start.1 = ((bf16[8,64,2048]{2,1,0:T(8,128)(2,1)}), bf16[8,64,2048]{2,1,0:T(8,128)(2,1)}, u32[]{:S(2)}, u32[]{:S(2)}) async-start(bf16[8,64,2048]{2,1,0:T(8,128)(2,1)} %bitcast.135), calls=%async_computation.2 | async-start | bytes 4194304 | tf_op jit(solution)/shard_map/all_to_all | solution.py:154
Sparse Core Ops, SparseCore 0:
  74.8 57.2 all-gather.1
  158.7 152.8 all-reduce.3
  314.1 260.6 reduce-scatter.4
where the time goes:
time: 611 us; the launch traced here: 609 us
  starting transfers between devices  241 us (39%)
  blocking collectives  157 us (26%)
  waiting for transfers between devices  88.2 us (14%)
  matrix products  44.3 us (7%)
  other arithmetic  33 us (5%)
  local copies, waits for them, and re-layouts  31.7 us (5%)
  between operations  14 us (2%)
    all_to_all x1, starting transfers between devices, on_device(): lax.all_to_all(summed.reshape(ep_size, local_experts * capacity, width),...  241 us
    all_gather x1, waiting for transfers between devices, on_device(): piece = lax.all_gather(arrived, 'tp', axis=0, tiled=True)  57.4 us
    all_to_all x1, blocking collectives, on_device(): lax.all_to_all(outgoing, 'ep', split_axis=1, concat_axis=1, tiled=True)  55.5 us
    all_gather x1, blocking collectives, on_device(): key_piece = lax.all_gather(key_rows, 'ep', axis=0, tiled=True)  34.8 us
    all_gather x1, blocking collectives, on_device(): value_piece = lax.all_gather(value_rows, 'ep', axis=0, tiled=True)  34 us
    all_gather x1, blocking collectives, on_device(): bias_piece = lax.all_gather(break_bias, 'ep', axis=0, tiled=True)  32.1 us
    another operation x4, other arithmetic  20 us
    reduce_scatter x1, waiting for transfers between devices, on_device(): lax.psum_scatter(jnp.dot(block, mixer_weight, preferred_element_type=jnp....  15.9 us
  transfers between devices with their start and end apart: 4, of which 4 were waited for; matrix products, arithmetic and copies ran while one was open for 9% of the time, Pallas kernels for 0%

commit v1 on v0

--- a/solution.py
+++ b/solution.py
@@ -78,8 +78,11 @@
     empty_totals = jnp.zeros((ep_size, heads_local, row_count), jnp.float32)
     empty_output = jnp.zeros((heads_local, row_count, DH), jnp.float32)
     empty_parts = jnp.zeros((ep_size, heads_local, row_count, DH), jnp.float32)
-    key_piece = lax.all_gather(key_rows, "ep", axis=0, tiled=True)
-    value_piece = lax.all_gather(value_rows, "ep", axis=0, tiled=True)
+    key_piece, value_piece = jnp.split(
+        lax.all_gather(jnp.concatenate([key_rows, value_rows], axis=1), "ep", axis=0, tiled=True),
+        [key_rows.shape[1]],
+        axis=1,
+    )
     bias_piece = lax.all_gather(break_bias, "ep", axis=0, tiled=True)
 
     def one_shard(index, current):

time: 611 us -> 557 us (0.912)
  waiting for transfers between devices: 88.2 us -> 186 us
  starting transfers between devices: 241 us -> 154 us
  blocking collectives: 157 us -> 87.9 us
    all_to_all x1, starting transfers between devices: 241 us -> 154 us  [on_device(): lax.all_to_all(summed.reshape(ep_size, local_experts * capacity, width),...]
    unnamed x4 -> x5, waiting for transfers between devices: 4.81 us -> 92.1 us
    all_gather x2 -> x0, blocking collectives: 68.9 us -> none  [the longest x1 34.8 us: on_device(): key_piece = lax.all_gather(key_rows, 'ep', axis=0, tiled=True)]
    all_to_all x1, waiting for transfers between devices: 10.2 us -> 21.5 us  [on_device(): lax.all_to_all(summed.reshape(ep_size, local_experts * capacity, width),...]
  transfers between devices with their start and end apart: 4 -> 5, of which waited for: 4 -> 4; matrix products, arithmetic and copies ran while one was open for 9% -> 15% of each run, Pallas kernels for 0% -> 0%
where the time goes in v1:
time: 557 us; the launch traced here: 555 us
  waiting for transfers between devices  186 us (33%)
  starting transfers between devices  154 us (28%)
  blocking collectives  87.9 us (16%)
  matrix products  44.3 us (8%)
  local copies, waits for them, and re-layouts  34.4 us (6%)
  other arithmetic  34 us (6%)
  between operations  14 us (3%)
    all_to_all x1, starting transfers between devices, on_device(): lax.all_to_all(summed.reshape(ep_size, local_experts * capacity, width),...  154 us
    unnamed x5, waiting for transfers between devices  92.1 us
    all_gather x1, waiting for transfers between devices, on_device(): piece = lax.all_gather(arrived, 'tp', axis=0, tiled=True)  56.3 us
    all_to_all x1, blocking collectives, on_device(): lax.all_to_all(outgoing, 'ep', split_axis=1, concat_axis=1, tiled=True)  55.5 us
    all_gather x1, blocking collectives, on_device(): bias_piece = lax.all_gather(break_bias, 'ep', axis=0, tiled=True)  32.4 us
    all_to_all x1, waiting for transfers between devices, on_device(): lax.all_to_all(summed.reshape(ep_size, local_experts * capacity, width),...  21.5 us
    another operation x4, other arithmetic  20 us
    reduce_scatter x1, waiting for transfers between devices, on_device(): lax.psum_scatter(jnp.dot(block, mixer_weight, preferred_element_type=jnp....  16.2 us
  transfers between devices with their start and end apart: 5, of which 4 were waited for; matrix products, arithmetic and copies ran while one was open for 15% of the time, Pallas kernels for 0%

profile of v1, /device:TPU:0, one launch (start us, length us, event | category | flops | bytes accessed | tf_op | source)
XLA Modules:
  0.0 555.2 jit_solution(3536465360401230055)
XLA Ops:
  7.2 0.8 broadcast_multiply_fusion
  8.1 0.1 copy.46
  8.2 0.1 eq.40
  8.3 0.1 eq.36
  8.5 0.6 reduce-window.28
  9.1 0.2 slice_reduce_fusion
  9.3 0.1 copy.45
  9.4 0.1 mul.145
  9.7 1.4 scatter_custom_fusion
  11.1 0.7 convert_element_type.85
  11.8 1.2 fusion.41
  13.0 1.2 fusion.43
  14.3 3.3 gather_fusion
  17.7 55.5 %all_to_all.10 = bf16[1,8,2,32,2048]{4,3,0,2,1:T(8,128)(2,1)S(1)} all-to-all(bf16[1,8,2,32,2048]{4,3,0,2,1:T(8,128)(2,1)} %bitcast.134), channel_id=1, replica_groups=mesh['ep'=8,'tp'=4] {'ep'}, dimensions={1} | all-to-all | bytes 4194304 | tf_op jit(solution)/shard_map/all_to_all | solution.py:141
  73.2 1.5 copy.50
  74.8 0.1 copy.42
  74.9 0.1 copy.43
  75.0 0.7 pad_maximum_fusion
  75.8 56.3 %all-gather.5.cloned.1.call-done = bf16[4,8,2,32,2048]{4,3,1,0,2:T(8,128)(2,1)} async-done(((bf16[1,8,2,32,2048]{4,3,1,0,2:T(8,128)(2,1)}), bf16[4,8,2,32,2048]{4,3,1,0,2:T(8,128)(2,1)}) %all-gather.5.cloned.1.call-update) | async-done | bytes 8388624 | tf_op jit(solution)/shard_map/all_gather | solution.py:142
  132.1 11.0 %fusion.26 = f32[2,4,8,32,512]{4,3,2,1,0:T(8,128)} fusion(bf16[4,8,2,32,2048]{4,3,1,0,2:T(8,128)(2,1)} %all-gather.5.cloned.1.call-done, bf16[2,2048,512]{2,1,0:T(8,128)(2,1)} %param.31), kind=kOutput, calls=%fused_computation.47 | convolution fusion | flops 4294967296 | bytes 16777216 | tf_op jit(solution)/shard_map/pnecd,edf->pnecf/dot_general | solution.py:146
  143.1 15.4 %convert_bitcast_fusion.2 = bf16[4,8,2,32,2048]{4,3,1,0,2:T(8,128)(2,1)} fusion(bf16[2,512,2048]{2,1,0:T(8,128)(2,1)} %param.32, f32[2,4,8,32,512]{4,3,2,1,0:T(8,128)} %fusion.26, bf16[4,8,2,32,2048]{4,3,1,0,2:T(8,128)(2,1)} %all-gather.5.cloned.1.call-done, bf16[2,2048,512]{2,1,0:T(8,128)(2,1)} %param.30), kind=kOutput, calls=%fused_computation.45 | convolution fusion | flops 8600420352 | bytes 29360128 | tf_op jit(solution)/shard_map/pnecf,efd->pnecd/dot_general | solution.py:150
  158.6 0.8 copy-done.4
  159.4 0.2 copy.44
  159.6 32.4 %all_gather.10 = bf16[3072,4]{0,1:T(4,128)(2,1)} all-gather(bf16[384,4]{0,1:T(4,128)(2,1)S(1)} %copy-done.8), channel_id=1, replica_groups=mesh['ep'=8,'tp'=4] {'ep'}, dimensions={0}, use_global_device_ids=true | all-gather | bytes 27648 | tf_op jit(solution)/shard_map/all_gather | solution.py:86
  192.0 2.7 fusion.61
  194.7 41.4 %while.18 = (s32[]{:T(128)}, f32[8,4,384,64]{2,3,1,0:T(8,128)}, f32[8,4,384]{2,1,0:T(4,128)S(1)}, s32[]{:T(128)}, s32[]{:T(128)}, /*index=5*/s32[]{:T(128)}, bf1...) while((s32[]{:T(128)}, f32[8,4,384,64]{2,3,1,0:T(8,128)}, ...), condition=%wide.region_6.7_spmd, body=%wide.region_0.6_spmd.sunk | while | flops 250984336 | bytes 43047352 | solution.py:112
  194.7 34.7 %conditional.2 = (f32[1,4,384,64]{2,3,1,0:T(8,128)S(1)}, f32[1,4,384]{2,1,0:T(4,128)S(1)}) conditional(s32[]{:T(128)} %convert_element_type.126, () %tuple.77, (s32[]{:T(128)}, s32[]{:T(128)}, bf16[3072,128]{0,1:T(8,128)(2,1)}, bf16[384,2,2,64]{0,3,2,1:T(8,128)(2,1)S(1)}, bf16[3072,4]{0,1:T(4,128)(2,1)}, /*index=5*/bf16[3072,128]{0,1:T(8,128)(2,1)}) %tuple.78), branch_computations={%region_1.1_spmd, %region_2.5_spmd} | conditional | flops 250984320 | bytes 42247824 | solution.py:107
  194.7 0.7 convert_bitcast_fusion.1
  195.4 1.0 constant_dynamic-slice_fusion
  196.4 0.1 broadcast_compare_fusion.1
  196.5 3.4 fusion.17
  199.9 0.1 copy.38
  200.1 0.3 broadcast_compare_fusion
  200.4 19.3 %fusion.2 = f32[4,384,3,128]{1,2,3,0:T(4,128)S(1)} fusion(f32[4,384,3,128]{1,3,2,0:T(8,128)} %bitcast.131, f32[4,3,128]{1,2,0:T(8,128)S(1)} %copy.38, pred[384,3,128]{0,1,2:T(4,128)(4,1)S(1)} %broadcast_compare_fusion), kind=kOutput, calls=%fused_computation.8 | output fusion | flops 80216064 | bytes 4872192 | tf_op jit(solution)/shard_map/reduce-window.10
  219.7 1.7 copy-done.1
  221.4 2.7 broadcast_add_fusion
  224.1 0.2 copy.40
  224.4 1.4 copy-done.2
  225.8 3.6 fusion.21
  229.4 0.8 constant_dynamic-update-slice_fusion.4
  230.2 0.8 constant_dynamic-update-slice_fusion.4
  231.1 0.8 constant_dynamic-update-slice_fusion.4
  231.9 0.8 constant_dynamic-update-slice_fusion.4
  232.8 0.8 constant_dynamic-update-slice_fusion.4
  233.6 0.8 constant_dynamic-update-slice_fusion.4
  234.5 0.8 constant_dynamic-update-slice_fusion.4
  235.3 0.8 constant_dynamic-update-slice_fusion.4
  236.2 2.3 multiply_reduce_fusion
  238.5 1.8 convolution_convert_fusion
  240.3 0.6 dynamic-slice
  240.9 92.1 %all-reduce.4.cloned.1.call-done = bf16[4,8,2,32,2048]{4,3,1,0,2:T(8,128)(2,1)} async-done(((bf16[4,8,2,32,2048]{4,3,1,0,2:T(8,128)(2,1)}), bf16[4,8,2,32,2048]{4,3,1,0,2:T(8,128)(2,1)}) %all-reduce.4.cloned.1.call-update) | async-done | bytes 8388624
  333.0 2.4 constant_dynamic-slice_fusion.2
  335.4 1.4 copy.51
  336.8 153.9 %all-to-all-start.1 = ((bf16[8,64,2048]{2,1,0:T(8,128)(2,1)}), bf16[8,64,2048]{2,1,0:T(8,128)(2,1)}, u32[]{:S(2)}, u32[]{:S(2)}) async-start(bf16[8,64,2048]{2,1,0:T(8,128)(2,1)} %bitcast.135), calls=%async_computation.2 | async-start | bytes 4194304 | tf_op jit(solution)/shard_map/all_to_all | solution.py:157
  490.7 0.2 copy.58
  490.9 2.0 fusion.63
  493.0 16.2 %reduce-scatter.5.cloned.1.call-done = bf16[96,2048]{1,0:T(8,128)(2,1)} async-done(((bf16[384,2048]{1,0:T(8,128)(2,1)}), bf16[96,2048]{1,0:T(8,128)(2,1)}) %reduce-scatter.5.cloned.1.call-update) | async-done | bytes 393232 | tf_op jit(solution)/shard_map/reduce_scatter | solution.py:119
  509.2 1.2 fusion.44
  510.3 1.9 fusion.46
  512.3 21.5 %all-to-all-done.1 = bf16[8,64,2048]{2,1,0:T(8,128)(2,1)} async-done(((bf16[8,64,2048]{2,1,0:T(8,128)(2,1)}), bf16[8,64,2048]{2,1,0:T(8,128)(2,1)}, u32[]{:S(2)}, u32[]{:S(2)}) %all-to-all-start.1) | async-done | bytes 2097184 | tf_op jit(solution)/shard_map/all_to_all | solution.py:157
  533.8 5.2 gather_fusion.1
  539.0 2.5 reshape.199
  541.5 3.5 fusion.62
  545.0 3.7 fusion.36
  (81 shorter events, 1.2 us)
Async XLA Ops:
  7.2 537.8 %copy-start = (bf16[512,2048]{1,0:T(8,128)(2,1)S(1)}, bf16[512,2048]{1,0:T(8,128)(2,1)}, u32[]{:S(2)}) copy-start(bf16[512,2048]{1,0:T(8,128)(2,1)} %param.35) | copy-start | bytes 6291460
  7.2 125.0 %all-gather.5.cloned.1.call-start = ((), (), s32[]{:S(2)}) async-start(), calls=%async_computation.5 | async-start | bytes 10485760 | tf_op jit(solution)/shard_map/all_gather | solution.py:142
  73.2 1.6 copy-start.5
  73.2 1.7 copy-start.6
  74.7 117.3 %all-gather.3.cloned.1.call-start = ((), (), s32[]{:S(2)}) async-start(), calls=%async_computation.3 | async-start | bytes 1769472 | tf_op jit(solution)/shard_map/all_gather | solution.py:82
  75.8 257.2 %all-reduce.4.cloned.1.call-start = ((), (), s32[]{:S(2)}) async-start(), calls=%async_computation.6 | async-start | bytes 16777216
  158.5 0.9 copy-start.4
  158.5 1.1 copy-start.8
  158.5 350.6 %reduce-scatter.5.cloned.1.call-start = ((), (), s32[]{:S(2)}) async-start(), calls=%async_computation.4 | async-start | bytes 1966080 | tf_op jit(solution)/shard_map/reduce_scatter | solution.py:119
  219.7 1.7 copy-start.1
  224.1 1.7 copy-start.2
  236.1 2.4 copy-start.3
  238.5 1.8 copy-start.10
  336.8 153.9 %copy-start.9 = (f32[128,2]{0,1:T(2,128)S(1)}, f32[128,2]{0,1:T(2,128)}, u32[]{:S(2)}) copy-start(f32[128,2]{0,1:T(2,128)} %param.29) | copy-start | bytes 3076
  336.8 154.1 %copy-start.7 = (bf16[2048]{0:T(1024)(128)(2,1)S(1)}, bf16[2048]{0:T(1024)(128)(2,1)}, u32[]{:S(2)}) copy-start(bf16[2048]{0:T(1024)(128)(2,1)} %param.25) | copy-start | bytes 12292
  336.8 196.9 %all-to-all-start.1 = ((bf16[8,64,2048]{2,1,0:T(8,128)(2,1)}), bf16[8,64,2048]{2,1,0:T(8,128)(2,1)}, u32[]{:S(2)}, u32[]{:S(2)}) async-start(bf16[8,64,2048]{2,1,0:T(8,128)(2,1)} %bitcast.135), calls=%async_computation.2 | async-start | bytes 4194304 | tf_op jit(solution)/shard_map/all_to_all | solution.py:157
Sparse Core Ops, SparseCore 0:
  74.8 57.2 all-gather.4
  134.8 44.6 all-gather.2
  181.9 151.0 all-reduce.3
  335.4 173.7 reduce-scatter.4
